TPU v7x, 32 devices: a whole 2x2x4 slice. The times are simulated.
32 devices in a mesh: ep: 8 (over z, x), tp: 4 (over y, core).
Axes of the slice: x: 2, y: 2, z: 4, core: 2. Of those that a mesh axis runs over, the one named last changes fastest.
Arguments:
- mix_query: bfloat16 [16384, 2048], P('ep', 'tp'), may hold values from -6 to 6
- mix_key: bfloat16 [16384, 2048], P('ep', 'tp'), may hold values from -6 to 6
- mix_value: bfloat16 [16384, 2048], P('ep', 'tp'), may hold values from -6 to 6
- mix_gate: bfloat16 [16384, 2048], P('ep', 'tp'), may hold values from -6 to 6
- log_decay: float32 [16384, 8], P('ep', 'tp'), may hold values from -1 to 0, as said below
- ret_gain: float32 [2048], P('tp'), may hold values from 0.1 to 1.9
- w_out: bfloat16 [2048, 2048], replicated, may hold values from -0.125 to 0.125
- moe_in: bfloat16 [1024, 2048], P(('ep', 'tp')), may hold values from -6 to 6
- route_ids: int32 [1024, 2], P(('ep', 'tp')), may hold values from 0 to 7, as said below
- route_weights: float32 [1024, 2], P(('ep', 'tp')), may hold values from 0.1 to 1
- moe_gain: float32 [2048], replicated, may hold values from 0.1 to 1.9
- w_gate: bfloat16 [8, 2048, 7168], P('ep', None, 'tp'), may hold values from -0.125 to 0.125
- w_up: bfloat16 [8, 2048, 7168], P('ep', None, 'tp'), may hold values from -0.125 to 0.125
- w_down: bfloat16 [8, 7168, 2048], P('ep', 'tp'), may hold values from -0.0625 to 0.0625
Outputs:
- mix_out: bfloat16 [16384, 2048], P(('ep', 'tp'))
- moe_out: bfloat16 [1024, 2048], P(('ep', 'tp'))
Inputs may be any that keep to these rules, and one draw needn't show every extreme that they name: `log_decay`: log of a decay. `route_ids`: each row names 2 different experts. Among the rows of one device no expert is named by more than 16 rows, and one expert is named by exactly 16 rows of every device.
All inputs are finite; a program needn't handle non-finite values.
Results may differ from a plain program's by a relative error of at most 0.015.
Values may be sent and summed in bfloat16 or wider, within the bound.
A program may use at most 128 MiB of HBM per device.

v0:
```python
import jax
import jax.numpy as jnp
from jax import lax
from jax.sharding import PartitionSpec as P

HEAD_DIM = 256
BLOCK = 512
norm_eps = 1e-06


def prefix(x, axis, join, neutral):
    place = lax.axis_index(axis)
    gathered = jax.tree.map(
        lambda a, kind: lax.all_gather(a.astype(kind), axis), x, (jnp.bfloat16, jnp.bfloat16)
    )
    state = jax.tree.map(lambda a, e: jnp.zeros_like(a) + jnp.asarray(e, a.dtype), x, neutral)

    def one(hop, state):
        return join(
            state,
            jax.tree.map(
                lambda a, own: lax.dynamic_index_in_dim(a, hop, 0, False).astype(own.dtype),
                gathered,
                x,
            ),
        )

    return lax.fori_loop(0, place, one, state)


def rotate(tensor, position_index):
    head_dim = tensor.shape[-1]
    half_dim = head_dim // 2
    inverse = 10000.0 ** (-(jnp.arange(half_dim, dtype=jnp.float32) * 2.0) / head_dim)
    angle = position_index.astype(jnp.float32)[:, None] * inverse[None, :]
    cosine = jnp.cos(angle)[:, None, :]
    sine = jnp.sin(angle)[:, None, :]
    front = tensor[..., :half_dim]
    back = tensor[..., half_dim:]
    return jnp.concatenate([front * cosine - back * sine, back * cosine + front * sine], axis=-1)


def chain(earlier, later):
    return (earlier[0] * later[0], later[0][:, None, None] * earlier[1] + later[1])


def carry_block(carried, block_items):
    update, block_last = block_items
    return (jnp.exp(block_last)[:, None, None] * carried + update, carried)


def mixer_half(mix_query, mix_key, mix_value, mix_gate, log_decay, ret_gain, w_out):
    seq_rows = mix_query.shape[0]
    local_heads = mix_query.shape[1] // HEAD_DIM
    block_count = seq_rows // BLOCK
    position_index = lax.axis_index("ep") * seq_rows + jnp.arange(seq_rows, dtype=jnp.int32)
    query_rot = rotate(
        mix_query.astype(jnp.float32).reshape(seq_rows, local_heads, HEAD_DIM), position_index
    ).astype(jnp.bfloat16)
    key_rot = (
        rotate(mix_key.astype(jnp.float32).reshape(seq_rows, local_heads, HEAD_DIM), position_index)
        * HEAD_DIM ** (-0.5)
    ).astype(jnp.bfloat16)
    query_blocks = query_rot.reshape(block_count, BLOCK, local_heads, HEAD_DIM)
    key_blocks = key_rot.reshape(block_count, BLOCK, local_heads, HEAD_DIM)
    value_blocks = mix_value.reshape(block_count, BLOCK, local_heads, HEAD_DIM)
    cumulative = jnp.cumsum(log_decay.reshape(block_count, BLOCK, local_heads), axis=1)
    causal = jnp.arange(BLOCK)[:, None] >= jnp.arange(BLOCK)[None, :]
    scores = jnp.einsum(
        "nihd,njhd->nhij", query_blocks, key_blocks, preferred_element_type=jnp.float32
    )
    by_head = jnp.transpose(cumulative, (0, 2, 1))
    log_gap = by_head[:, :, :, None] - by_head[:, :, None, :]
    decay_mask = jnp.where(causal, jnp.exp(jnp.where(causal, log_gap, 0.0)), 0.0)
    weights = (scores * decay_mask).astype(jnp.bfloat16)
    within_block = jnp.einsum(
        "nhij,njhe->nihe", weights, value_blocks, preferred_element_type=jnp.float32
    )
    block_last = cumulative[:, -1, :]
    key_decayed = (
        key_blocks.astype(jnp.float32) * jnp.exp(block_last[:, None, :] - cumulative)[..., None]
    ).astype(jnp.bfloat16)
    updates = jnp.einsum(
        "njhd,njhe->nhde", key_decayed, value_blocks, preferred_element_type=jnp.float32
    )
    empty_state = jnp.zeros((local_heads, HEAD_DIM, HEAD_DIM), jnp.float32)
    local_end, starts = lax.scan(carry_block, empty_state, (updates, block_last))
    through = jnp.cumsum(block_last, axis=0)
    before = through - block_last
    incoming = prefix(
        (jnp.exp(through[-1]), local_end), "ep", chain, (jnp.ones_like(through[-1]), empty_state)
    )
    block_states = starts + jnp.exp(before)[:, :, None, None] * incoming[1][None]
    query_decayed = query_blocks.astype(jnp.float32) * jnp.exp(cumulative)[..., None]
    carried_part = jnp.einsum(
        "nihd,nhde->nihe", query_decayed, block_states, precision=lax.Precision.HIGHEST
    )
    retained = (within_block + carried_part).reshape(seq_rows, local_heads, HEAD_DIM)
    inverse_rms = lax.rsqrt(jnp.mean(retained * retained, axis=-1, keepdims=True) + norm_eps)
    gate_act = jax.nn.silu(mix_gate.astype(jnp.float32).reshape(seq_rows, local_heads, HEAD_DIM))
    heads_out = (
        gate_act * retained * inverse_rms * ret_gain.reshape(local_heads, HEAD_DIM)
    ).astype(jnp.bfloat16)
    by_rows = lax.all_to_all(
        heads_out.reshape(seq_rows, local_heads * HEAD_DIM),
        "tp",
        split_axis=0,
        concat_axis=1,
        tiled=True,
    )
    return jnp.dot(by_rows, w_out, preferred_element_type=jnp.float32).astype(jnp.bfloat16)


def expert_half(moe_in, route_ids, route_weights, moe_gain, w_gate, w_up, w_down):
    tokens, model_width = moe_in.shape
    route_count = route_ids.shape[1]
    experts = lax.axis_size("ep")
    lane_count = lax.axis_size("tp")
    capacity = 4 * tokens // experts
    floats = moe_in.astype(jnp.float32)
    normed = (
        floats * lax.rsqrt(jnp.mean(floats * floats, axis=-1, keepdims=True) + norm_eps) * moe_gain
    ).astype(jnp.bfloat16)
    flat_ids = route_ids.reshape(-1)
    onehot = (flat_ids[:, None] == jnp.arange(experts, dtype=jnp.int32)[None, :]).astype(jnp.int32)
    slot_index = jnp.sum(jnp.cumsum(onehot, axis=0) * onehot, axis=1) - 1
    target = flat_ids * capacity + slot_index
    source = jnp.arange(tokens * route_count, dtype=jnp.int32) // route_count
    slot_owner = jnp.full((experts * capacity,), tokens, jnp.int32).at[target].set(source)
    padded = jnp.concatenate([normed, jnp.zeros((1, model_width), jnp.bfloat16)], axis=0)
    outgoing = padded[slot_owner]
    gate_weight = w_gate[0]
    up_weight = w_up[0]
    down_weight = w_down[0]
    copies = jnp.broadcast_to(
        outgoing.reshape(experts, 1, capacity, model_width),
        (experts, lane_count, capacity, model_width),
    )
    arrived = lax.all_to_all(
        copies.reshape(experts * lane_count * capacity, model_width),
        ("ep", "tp"),
        split_axis=0,
        concat_axis=0,
        tiled=True,
    )
    gate_part = jnp.dot(arrived, gate_weight, preferred_element_type=jnp.float32)
    up_part = jnp.dot(arrived, up_weight, preferred_element_type=jnp.float32)
    hidden_grid = (
        (jax.nn.silu(gate_part) * up_part)
        .astype(jnp.bfloat16)
        .reshape(experts, lane_count, capacity, -1)
    )
    partial_value = jnp.einsum(
        "elcf,fd->lecd", hidden_grid, down_weight, preferred_element_type=jnp.float32
    )
    summed_rows = lax.psum_scatter(
        partial_value.reshape(lax.axis_size("tp") * (experts * capacity), model_width).astype(
            jnp.bfloat16
        ),
        "tp",
        scatter_dimension=0,
        tiled=True,
    )
    returned = lax.all_to_all(summed_rows, "ep", split_axis=0, concat_axis=0, tiled=True)
    picked_rows = returned[target].reshape(tokens, route_count, model_width)
    combined = jnp.sum(picked_rows.astype(jnp.float32) * route_weights[:, :, None], axis=1)
    return combined.astype(jnp.bfloat16)


def on_device(
    mix_query,
    mix_key,
    mix_value,
    mix_gate,
    log_decay,
    ret_gain,
    w_out,
    moe_in,
    route_ids,
    route_weights,
    moe_gain,
    w_gate,
    w_up,
    w_down,
):
    mix_out = mixer_half(mix_query, mix_key, mix_value, mix_gate, log_decay, ret_gain, w_out)
    moe_out = expert_half(moe_in, route_ids, route_weights, moe_gain, w_gate, w_up, w_down)
    return (mix_out, moe_out)


def solution(mesh):
    in_specs = (
        P("ep", "tp"),
        P("ep", "tp"),
        P("ep", "tp"),
        P("ep", "tp"),
        P("ep", "tp"),
        P("tp"),
        P(),
        P(("ep", "tp"), None),
        P(("ep", "tp"), None),
        P(("ep", "tp"), None),
        P(),
        P("ep", None, "tp"),
        P("ep", None, "tp"),
        P("ep", "tp", None),
    )
    out_specs = (P(("ep", "tp"), None), P(("ep", "tp"), None))
    return jax.shard_map(
        on_device, mesh=mesh, in_specs=in_specs, out_specs=out_specs, check_vma=False
    )
```

profile of v0, /device:TPU:0, one launch (start us, length us, event | category | flops | bytes accessed | tf_op | source)
XLA Modules:
  0.0 214.7 jit_solution(8959980904177569203)
XLA Ops:
  15.6 7.5 %all-to-all-start.1 = ((bf16[32,16,2048]{2,1,0:T(8,128)(2,1)}), bf16[32,16,2048]{2,1,0:T(8,128)(2,1)}, u32[]{:S(2)}, u32[]{:S(2)}) async-start(bf16[32,16,2048]{2,1,0:T(8,128)(2,1)} %bitcast.23), calls=%async_computation.1 | async-start | bytes 4194304 | tf_op jit(solution)/shard_map/all_to_all | solution.py:139
  26.9 2.9 %copy.165 = bf16[2048,512]{0,1:T(8,128)(2,1)S(1)} copy(bf16[2048,512]{1,0:T(8,128)(2,1)} %param.18) | data formatting | bytes 4194304 | tf_op args[0]
  29.8 2.5 %convert.15 = f32[2048,2,256]{0,2,1:T(8,128)} convert(bf16[2048,2,256]{0,2,1:T(8,128)(2,1)S(1)} %bitcast.104) | non-fusion elementwise | flops 1048576 | bytes 6291456 | tf_op jit(solution)/shard_map/reshape | solution.py:58
  32.3 2.9 %copy.170 = bf16[2048,512]{0,1:T(8,128)(2,1)S(1)} copy(bf16[2048,512]{1,0:T(8,128)(2,1)} %param.19) | data formatting | bytes 4194304 | tf_op args[1]
  35.7 3.7 %multiply_cosine_fusion = (f32[2048,128]{0,1:T(8,128)S(1)}, f32[2048,128]{0,1:T(8,128)S(1)}) fusion(f32[128]{0:T(128)S(1)} %multiply_power_fusion, f32[2048]{0:T(1024)S(1)} %add_convert_fusion.1), kind=kLoop, calls=%fused_computation.61 | loop fusion | flops 262144 | bytes 2105856 | tf_op jit(solution)/shard_map/cos | solution.py:36
  39.5 3.1 %multiply_subtract_fusion = (f32[2048,2,128]{0,2,1:T(8,128)}, f32[2048,2,128]{0,2,1:T(8,128)S(1)}, bf16[2048,2,128]{0,2,1:T(8,128)(2,1)S(1)}, bf16[2048,2,128]{0,2,1:T(8,128)(2,1)}) fusion(f32[2048,2,256]{0,2,1:T(8,128)S(1)} %convert.16, f32[2048,128]{0,1:T(8,128)S(1)} %get-tuple-element.194, f32[2048,128]{0,1:T(8,128)S(1)} %get-tuple-element.193, ...), kind=kLoop, calls=%fused_computation.53 | loop fusion | flops 7340032 | bytes 16777216 | tf_op jit(solution)/shard_map/sub | solution.py:40
  42.5 2.9 %copy.171 = f32[2048,2,128]{2,0,1:T(8,128)} copy(f32[2048,2,128]{0,2,1:T(8,128)} %get-tuple-element.185) | data formatting | bytes 4194304 | tf_op jit(solution)/shard_map/sub | solution.py:40
  47.3 4.2 %reshape.244 = bf16[4,512,2,256]{3,2,1,0:T(2,128)(2,1)} reshape(bf16[2048,512]{1,0:T(8,128)(2,1)} %param.20) | data formatting | bytes 4194304 | tf_op jit(solution)/shard_map/reshape | solution.py:66
  51.4 5.1 %fusion.36 = f32[4,2,256,256]{3,2,1,0:T(8,128)} fusion(f32[4,512,2]{1,2,0:T(2,128)S(1)} %copy.180, bf16[4,512,2,256]{3,2,1,0:T(2,128)(2,1)} %reshape.244, f32[4,512,2,128]{3,1,0,2:T(8,128)} %bitcast.115, f32[4,512,2,128]{3,1,0,2:T(8,128)S(1)} %bitcast.114), kind=kOutput, calls=%fused_computation.46 | convolution fusion | flops 543162368 | bytes 8404992 | tf_op jit(solution)/shard_map/njhd,njhe->nhde/dot_general | solution.py:83
  56.6 8.1 %while.26 = (s32[]{:T(128)}, f32[2,256,256]{2,1,0:T(8,128)S(1)}, f32[4,2,256,256]{3,2,1,0:T(8,128)}, f32[4,2]{1,0:T(4,128)S(1)}, f32[4,2,256,256]{3,2,1,0:T(8,128)}, /*index=5*/s32[]{:T(128)}, s32[]{:T(128)}) while((s32[]{:T(128)}, f32[2,256,256]{2,1,0:T(8,128)S(1)}, f32[4,2,256,256]{3,2,1,0:T(8,128)}, f32[4,2]{1,0:T(4,128)S(1)}, ...), condition=%wide.region_3.4_spmd.clone, body=%wide.region_2.3_spmd.clone.sunk | while | flops 524291 | bytes 2622072 | solution.py:87
  65.9 20.9 %all-gather.1 = bf16[8,1,2]{2,1,0:T(2,128)(2,1)S(1)} all-gather(bf16[1,1,2]{2,1,0:T(2,128)(2,1)S(1)} %bitcast.125), channel_id=1, replica_groups=mesh['ep'=8,'tp'=4] {'ep'}, dimensions={0}, use_global_device_ids=true | all-gather | bytes 36 | tf_op jit(solution)/shard_map/all_gather | solution.py:14
  88.4 7.5 %fusion.14 = f32[4,2,512,256]{2,3,1,0:T(8,128)} fusion(f32[4,2,512]{2,1,0:T(2,128)S(1)} %reshape.284, pred[512,512]{1,0:T(8,128)(4,1)S(1)} %iota_compare_fusion, bf16[4,512,2,256]{3,2,1,0:T(2,128)(2,1)} %reshape.244, f32[4,512,2,128]{3,1,0,2:T(8,128)} %bitcast.116, f32[4,512,2,128]{3,1,0,2:T(8,128)} %bitcast.113, ...), kind=kOutput, calls=%fused_computation.26 | convolution fusion | flops 2165309440 | bytes 12861440 | tf_op jit(solution)/shard_map/nhij,njhe->nihe/dot_general | solution.py:76
  95.9 7.8 %fusion.6 = f32[512,1792]{1,0:T(8,128)S(1)} fusion(bf16[512,2048]{1,0:T(8,128)(2,1)} %bitcast.24, bf16[1,2048,1792]{2,1,0:T(8,128)(2,1)} %param.29), kind=kOutput, calls=%fused_computation.16 | convolution fusion | flops 3758096384 | bytes 13107200 | tf_op jit(solution)/shard_map/dot_general | solution.py:146
  103.8 8.0 %multiply_convert_fusion.3 = bf16[512,1792]{1,0:T(8,128)(2,1)S(1)} fusion(f32[512,1792]{1,0:T(8,128)S(1)} %fusion.6, bf16[512,2048]{1,0:T(8,128)(2,1)} %bitcast.24, bf16[1,2048,1792]{2,1,0:T(8,128)(2,1)} %param.30), kind=kOutput, calls=%fused_computation.41 | convolution fusion | flops 3763601408 | bytes 14942208 | tf_op jit(solution)/shard_map/dot_general | solution.py:147
  111.9 4.2 %fusion.31 = bf16[4,8,16,2048]{3,2,0,1:T(8,128)(2,1)S(1)} fusion(bf16[8,4,16,1792]{3,2,1,0:T(8,128)(2,1)S(1)} %bitcast.128, bf16[1,1792,2048]{2,1,0:T(8,128)(2,1)S(1)} %bitcast.127), kind=kOutput, calls=%fused_computation.45 | convolution fusion | flops 3759144960 | bytes 11272192 | tf_op jit(solution)/shard_map/elcf,fd->lecd/dot_general | solution.py:153
  118.0 11.4 %multiply_reduce_fusion = (f32[4,512,2]{1,2,0:T(2,128)S(1)}, f32[4,512,2,256]{1,3,2,0:T(8,128)}) fusion(f32[4,512,2]{1,2,0:T(2,128)S(1)} %copy.187, f32[4,2,256,256]{3,2,1,0:T(8,128)} %get-tuple-element.74, f32[2,256,256]{2,1,0:T(8,128)S(1)} %get-tuple-element.76, f32[4,2]{1,0:T(4,128)S(1)} %copy.184, f32[4,2,512,256]{2,3,1,0:T(8,128)} %fusion.14, ...), kind=kOutput, calls=%fused_computation.31 | convolution fusion | flops 3231707136 | bytes 13140000 | tf_op jit(solution)/shard_map/nihd,nhde->nihe/dot_general | solution.py:95
  129.8 2.5 %mul.264 = f32[2048,2,256]{2,1,0:T(2,128)S(1)} broadcast(f32[2048,2]{1,0:T(8,128)S(1)} %copy.190), dimensions={0,1} | broadcast | bytes 4210688 | tf_op jit(solution)/shard_map/mul | solution.py:102
  134.7 7.3 %copy.189 = f32[4,512,2,256]{3,2,1,0:T(2,128)} copy(f32[4,512,2,256]{1,3,2,0:T(8,128)} %get-tuple-element.196) | data formatting | bytes 8388608 | tf_op jit(solution)/shard_map/add | solution.py:98
  142.0 2.8 %copy.204 = f32[256,8,2,256]{3,1,2,0:T(8,128)S(1)} copy(f32[256,8,2,256]{3,2,1,0:T(2,128)} %bitcast.102) | data formatting | bytes 8388608
  150.2 3.7 %all-to-all-start = ((bf16[4,512,512]{1,2,0:T(8,128)(2,1)}), bf16[4,512,512]{1,2,0:T(8,128)(2,1)S(1)}, u32[]{:S(2)}, u32[]{:S(2)}) async-start(bf16[4,512,512]{1,2,0:T(8,128)(2,1)} %copy.191), calls=%async_computation | async-start | bytes 4194304 | tf_op jit(solution)/shard_map/all_to_all | solution.py:104
  154.0 25.5 %all-to-all-done = bf16[4,512,512]{1,2,0:T(8,128)(2,1)S(1)} async-done(((bf16[4,512,512]{1,2,0:T(8,128)(2,1)}), bf16[4,512,512]{1,2,0:T(8,128)(2,1)S(1)}, u32[]{:S(2)}, u32[]{:S(2)}) %all-to-all-start) | async-done | bytes 2097184 | tf_op jit(solution)/shard_map/all_to_all | solution.py:104
  179.5 11.0 %all-to-all-start.2 = ((bf16[8,16,2048]{2,1,0:T(8,128)(2,1)}), bf16[8,16,2048]{2,1,0:T(8,128)(2,1)S(1)}, u32[]{:S(2)}, u32[]{:S(2)}) async-start(bf16[8,16,2048]{2,1,0:T(8,128)(2,1)} %bitcast.119), calls=%async_computation.3 | async-start | bytes 1048576 | tf_op jit(solution)/shard_map/all_to_all | solution.py:164
  190.5 9.1 %convolution_convert_fusion = bf16[512,2048]{1,0:T(8,128)(2,1)} fusion(bf16[512,2048]{0,1:T(8,128)(2,1)S(1)} %bitcast.117, bf16[2048,2048]{1,0:T(8,128)(2,1)} %param.24), kind=kOutput, calls=%fused_computation.43 | convolution fusion | flops 4296015872 | bytes 12582912 | tf_op jit(solution)/shard_map/dot_general | solution.py:111
  199.7 5.1 %all-to-all-done.2 = bf16[8,16,2048]{2,1,0:T(8,128)(2,1)S(1)} async-done(((bf16[8,16,2048]{2,1,0:T(8,128)(2,1)}), bf16[8,16,2048]{2,1,0:T(8,128)(2,1)S(1)}, u32[]{:S(2)}, u32[]{:S(2)}) %all-to-all-start.2) | async-done | bytes 524320 | tf_op jit(solution)/shard_map/all_to_all | solution.py:164
  (101 shorter events, 37.2 us)
Async XLA Ops:
  15.6 7.5 %copy-start.5 = (f32[2048,2]{0,1:T(2,128)S(1)}, f32[2048,2]{0,1:T(2,128)}, u32[]{:S(2)}) copy-start(f32[2048,2]{0,1:T(2,128)} %param.22) | copy-start | bytes 49156
  15.6 80.4 %all-to-all-start.1 = ((bf16[32,16,2048]{2,1,0:T(8,128)(2,1)}), bf16[32,16,2048]{2,1,0:T(8,128)(2,1)}, u32[]{:S(2)}, u32[]{:S(2)}) async-start(bf16[32,16,2048]{2,1,0:T(8,128)(2,1)} %bitcast.23), calls=%async_computation.1 | async-start | bytes 4194304 | tf_op jit(solution)/shard_map/all_to_all | solution.py:139
  23.0 94.6 %all-gather.4.cloned.1.call-start = ((), (), s32[]{:S(2)}) async-start(), calls=%async_computation.5 | async-start | bytes 2359296 | tf_op jit(solution)/shard_map/all_gather | solution.py:14
  35.2 4.2 %copy-start.1 = (f32[2048,2,256]{0,2,1:T(8,128)S(1)}, f32[2048,2,256]{0,2,1:T(8,128)}, u32[]{:S(2)}) copy-start(f32[2048,2,256]{0,2,1:T(8,128)} %convert.15) | copy-start | bytes 12582916
  47.3 4.2 %copy-start.3 = (f32[2048,2,128]{2,0,1:T(8,128)S(1)}, f32[2048,2,128]{2,0,1:T(8,128)}, u32[]{:S(2)}) copy-start(f32[2048,2,128]{2,0,1:T(8,128)} %copy.171) | copy-start | bytes 6291460
  56.6 30.3 %copy-start.2 = (bf16[2048,2,128]{0,2,1:T(8,128)(2,1)S(1)}, bf16[2048,2,128]{0,2,1:T(8,128)(2,1)}, u32[]{:S(2)}) copy-start(bf16[2048,2,128]{0,2,1:T(8,128)(2,1)} %get-tuple-element.190) | copy-start | bytes 3145732
  65.4 114.1 %reduce-scatter.2.cloned.1.call-start = ((), (), s32[]{:S(2)}) async-start(), calls=%async_computation.4 | async-start | bytes 2621440 | tf_op jit(solution)/shard_map/reduce_scatter | solution.py:156
  95.9 15.9 %slice-start = ((s8[7340032]{0:T(1024)(128)(4,1)}), s8[4194304]{0:T(1024)(128)(4,1)S(1)}, s32[]{:S(2)}) async-start(s8[7340032]{0:T(1024)(128)(4,1)} %bitcast.126), calls=%async_computation.6 | async-start | bytes 8388608
  103.8 8.1 %slice-start.1 = ((s8[7340032]{0:T(1024)(128)(4,1)}), s8[3145728]{0:T(1024)(128)(4,1)S(1)}, s32[]{:S(2)}) async-start(s8[7340032]{0:T(1024)(128)(4,1)} %bitcast.126), calls=%async_computation.7 | async-start | bytes 6291456
  142.0 3.5 %copy-start = (f32[256,8,2,256]{3,1,2,0:T(8,128)S(1)}, f32[256,8,2,256]{3,1,2,0:T(8,128)}, u32[]{:S(2)}) copy-start(f32[256,8,2,256]{3,1,2,0:T(8,128)} %copy.205) | copy-start | bytes 12582916
  142.0 4.2 %copy-start.4 = (bf16[2048,512]{1,0:T(8,128)(2,1)S(1)}, bf16[2048,512]{1,0:T(8,128)(2,1)}, u32[]{:S(2)}) copy-start(bf16[2048,512]{1,0:T(8,128)(2,1)} %param.21) | copy-start | bytes 6291460
  142.0 4.2 %copy-start.6 = (f32[512]{0:T(512)S(1)}, f32[512]{0:T(512)}, u32[]{:S(2)}) copy-start(f32[512]{0:T(512)} %param.23) | copy-start | bytes 6148
  150.2 3.8 %copy-start.7 = (f32[32,2]{0,1:T(2,128)S(1)}, f32[32,2]{0,1:T(2,128)}, u32[]{:S(2)}) copy-start(f32[32,2]{0,1:T(2,128)} %param.27) | copy-start | bytes 772
  150.2 29.4 %all-to-all-start = ((bf16[4,512,512]{1,2,0:T(8,128)(2,1)}), bf16[4,512,512]{1,2,0:T(8,128)(2,1)S(1)}, u32[]{:S(2)}, u32[]{:S(2)}) async-start(bf16[4,512,512]{1,2,0:T(8,128)(2,1)} %copy.191), calls=%async_computation | async-start | bytes 4194304 | tf_op jit(solution)/shard_map/all_to_all | solution.py:104
  179.5 25.2 %all-to-all-start.2 = ((bf16[8,16,2048]{2,1,0:T(8,128)(2,1)}), bf16[8,16,2048]{2,1,0:T(8,128)(2,1)S(1)}, u32[]{:S(2)}, u32[]{:S(2)}) async-start(bf16[8,16,2048]{2,1,0:T(8,128)(2,1)} %bitcast.119), calls=%async_computation.3 | async-start | bytes 1048576 | tf_op jit(solution)/shard_map/all_to_all | solution.py:164
Sparse Core Ops, SparseCore 0:
  65.6 50.4 all-gather.3
Sparse Core Ops, SparseCore 1:
  117.7 28.5 reduce-scatter.1
where the time goes:
time: 216 us; the launch traced here: 215 us
  matrix products  53.2 us (25%)
  local copies, waits for them, and re-layouts  43.1 us (20%)
  waiting for transfers between devices  30.7 us (14%)
  other arithmetic  28.4 us (13%)
  starting transfers between devices  22.3 us (10%)
  blocking collectives  20.9 us (10%)
  between operations  15.9 us (7%)
    all_to_all x1, waiting for transfers between devices, mixer_half(): lax.all_to_all(heads_out.reshape(seq_rows, local_heads * HEAD_DIM), 'tp',...  25.5 us
    all_gather x1, blocking collectives, prefix(): lax.all_gather(a.astype(kind), axis)  20.9 us
    unnamed x27, local copies, waits for them, and re-layouts  13.4 us
    dot_general x1, matrix products, mixer_half(): jnp.einsum('nihd,nhde->nihe', query_decayed, block_states, precision=lax....  11.4 us
    all_to_all x1, starting transfers between devices, expert_half(): lax.all_to_all(summed_rows, 'ep', split_axis=0, concat_axis=0, tiled=True)  11 us
    dot_general x1, matrix products, mixer_half(): jnp.dot(by_rows, w_out, preferred_element_type=jnp.float32)  9.11 us
    dot_general x1, matrix products, expert_half(): up_part = jnp.dot(arrived, up_weight, preferred_element_type=jnp.float32)  8.03 us
    dot_general x1, matrix products, expert_half(): jnp.dot(arrived, gate_weight, preferred_element_type=jnp.float32)  7.83 us
  transfers between devices with their start and end apart: 5, of which 2 were waited for; matrix products, arithmetic and copies ran while one was open for 53% of the time, Pallas kernels for 0%

commit v1 on v0

--- a/solution.py
+++ b/solution.py
@@ -1,3 +1,4 @@
+import functools
 import jax
 import jax.numpy as jnp
 from jax import lax
@@ -6,6 +7,22 @@
 HEAD_DIM = 256
 BLOCK = 512
 norm_eps = 1e-06
+
+
+def treat_waves_now(x_local, array_axis, pos_dim):
+    answer = jnp.concatenate(
+        jax.lax.all_to_all(
+            jnp.stack(jnp.split(x_local, jax.lax.axis_size("tp"), axis=array_axis), axis=0),
+            "tp",
+            split_axis=0,
+            concat_axis=0,
+        ),
+        axis=pos_dim,
+    )
+    return answer
+
+
+state_the_stops_all = functools.partial(treat_waves_now, array_axis=0, pos_dim=1)
 
 
 def prefix(x, axis, join, neutral):
@@ -101,13 +118,7 @@
     heads_out = (
         gate_act * retained * inverse_rms * ret_gain.reshape(local_heads, HEAD_DIM)
     ).astype(jnp.bfloat16)
-    by_rows = lax.all_to_all(
-        heads_out.reshape(seq_rows, local_heads * HEAD_DIM),
-        "tp",
-        split_axis=0,
-        concat_axis=1,
-        tiled=True,
-    )
+    by_rows = state_the_stops_all(heads_out.reshape(seq_rows, local_heads * HEAD_DIM))
     return jnp.dot(by_rows, w_out, preferred_element_type=jnp.float32).astype(jnp.bfloat16)
 
 

time: 216 us -> 209 us (0.968)
  local copies, waits for them, and re-layouts: 43.1 us -> 35.4 us
  other arithmetic: 28.4 us -> 32.2 us
    reshape x2 -> x3, local copies, waits for them, and re-layouts: 0.03 us -> 5.44 us  [the longest x1 5.42 us: mixer_half(): (within_block + carried_part).reshape(seq_rows, local_heads, HEAD_DIM)]
    add x1, local copies, waits for them, and re-layouts: 7.27 us -> 2.2 us  [mixer_half(): within_block + carried_part]
    unnamed x27 -> x24, local copies, waits for them, and re-layouts: 13.4 us -> 9.78 us
    mul x1, local copies, waits for them, and re-layouts: 2.46 us -> 0.01 us  [mixer_half(): gate_act * retained * inverse_rms * ret_gain.reshape(local_heads, HEAD_DIM)]
    all_to_all x1 -> x0, local copies, waits for them, and re-layouts: 2.36 us -> none  [mixer_half(): lax.all_to_all(heads_out.reshape(seq_rows, local_heads * HEAD_DIM), 'tp',...]
    convert_element_type x1, other arithmetic: 1.65 us -> 3.84 us  [mixer_half(): heads_out = (gate_act * retained * inverse_rms * ret_gain.reshape(local_h...]
    another operation x3 -> x4, other arithmetic: 3.22 us -> 4.8 us
  transfers between devices with their start and end apart: 5 -> 5, of which waited for: 2 -> 2; matrix products, arithmetic and copies ran while one was open for 53% -> 52% of each run, Pallas kernels for 0% -> 0%
where the time goes in v1:
time: 209 us; the launch traced here: 208 us
  matrix products  51.1 us (24%)
  local copies, waits for them, and re-layouts  35.4 us (17%)
  other arithmetic  32.2 us (15%)
  waiting for transfers between devices  30.7 us (15%)
  starting transfers between devices  21.4 us (10%)
  blocking collectives  20.9 us (10%)
  between operations  15.9 us (8%)
    all_to_all x1, waiting for transfers between devices, treat_waves_now(): jax.lax.all_to_all(jnp.stack(jnp.split(x_local, jax.lax.axis_size('tp'),...  25.5 us
    all_gather x1, blocking collectives, prefix(): lax.all_gather(a.astype(kind), axis)  20.9 us
    all_to_all x1, starting transfers between devices, expert_half(): lax.all_to_all(summed_rows, 'ep', split_axis=0, concat_axis=0, tiled=True)  10.1 us
    unnamed x24, local copies, waits for them, and re-layouts  9.78 us
    dot_general x1, matrix products, mixer_half(): jnp.einsum('nihd,nhde->nihe', query_decayed, block_states, precision=lax....  9.33 us
    dot_general x1, matrix products, mixer_half(): jnp.dot(by_rows, w_out, preferred_element_type=jnp.float32)  9.11 us
    dot_general x1, matrix products, expert_half(): up_part = jnp.dot(arrived, up_weight, preferred_element_type=jnp.float32)  8.06 us
    dot_general x1, matrix products, expert_half(): jnp.dot(arrived, gate_weight, preferred_element_type=jnp.float32)  7.84 us
  transfers between devices with their start and end apart: 5, of which 2 were waited for; matrix products, arithmetic and copies ran while one was open for 52% of the time, Pallas kernels for 0%

profile of v1, /device:TPU:0, one launch (start us, length us, event | category | flops | bytes accessed | tf_op | source)
XLA Modules:
  0.0 208.0 jit_solution(11516267147990734243)
XLA Ops:
  15.6 7.5 %all-to-all-start.1 = ((bf16[32,16,2048]{2,1,0:T(8,128)(2,1)}), bf16[32,16,2048]{2,1,0:T(8,128)(2,1)}, u32[]{:S(2)}, u32[]{:S(2)}) async-start(bf16[32,16,2048]{2,1,0:T(8,128)(2,1)} %bitcast.29), calls=%async_computation.1 | async-start | bytes 4194304 | tf_op jit(solution)/shard_map/all_to_all | solution.py:150
  26.9 2.9 %copy.143 = bf16[2048,512]{0,1:T(8,128)(2,1)S(1)} copy(bf16[2048,512]{1,0:T(8,128)(2,1)} %param.18) | data formatting | bytes 4194304 | tf_op args[0]
  29.8 2.5 %convert.17 = f32[2048,2,256]{0,2,1:T(8,128)} convert(bf16[2048,2,256]{0,2,1:T(8,128)(2,1)S(1)} %bitcast.103) | non-fusion elementwise | flops 1048576 | bytes 6291456 | tf_op jit(solution)/shard_map/reshape | solution.py:75
  32.3 2.9 %copy.148 = bf16[2048,512]{0,1:T(8,128)(2,1)S(1)} copy(bf16[2048,512]{1,0:T(8,128)(2,1)} %param.19) | data formatting | bytes 4194304 | tf_op args[1]
  35.7 3.7 %multiply_cosine_fusion = (f32[2048,128]{0,1:T(8,128)S(1)}, f32[2048,128]{0,1:T(8,128)S(1)}) fusion(f32[128]{0:T(128)S(1)} %multiply_power_fusion, f32[2048]{0:T(1024)S(1)} %add_convert_fusion.1), kind=kLoop, calls=%fused_computation.62 | loop fusion | flops 262144 | bytes 2105856 | tf_op jit(solution)/shard_map/cos | solution.py:53
  39.5 3.1 %multiply_subtract_fusion = (f32[2048,2,128]{0,2,1:T(8,128)}, f32[2048,2,128]{0,2,1:T(8,128)S(1)}, bf16[2048,2,128]{0,2,1:T(8,128)(2,1)S(1)}, bf16[2048,2,128]{0,2,1:T(8,128)(2,1)}) fusion(f32[2048,2,256]{0,2,1:T(8,128)S(1)} %convert.18, f32[2048,128]{0,1:T(8,128)S(1)} %get-tuple-element.188, f32[2048,128]{0,1:T(8,128)S(1)} %get-tuple-element.187, ...), kind=kLoop, calls=%fused_computation.54 | loop fusion | flops 7340032 | bytes 16777216 | tf_op jit(solution)/shard_map/sub | solution.py:57
  42.5 2.9 %copy.149 = f32[2048,2,128]{2,0,1:T(8,128)} copy(f32[2048,2,128]{0,2,1:T(8,128)} %get-tuple-element.175) | data formatting | bytes 4194304 | tf_op jit(solution)/shard_map/sub | solution.py:57
  47.3 4.2 %reshape.258 = bf16[4,512,2,256]{3,2,1,0:T(2,128)(2,1)} reshape(bf16[2048,512]{1,0:T(8,128)(2,1)} %param.20) | data formatting | bytes 4194304 | tf_op jit(solution)/shard_map/reshape | solution.py:83
  51.4 5.1 %fusion.36 = f32[4,2,256,256]{3,2,1,0:T(8,128)} fusion(f32[4,512,2]{1,2,0:T(2,128)S(1)} %copy.158, bf16[4,512,2,256]{3,2,1,0:T(2,128)(2,1)} %reshape.258, f32[4,512,2,128]{3,1,0,2:T(8,128)} %bitcast.113, f32[4,512,2,128]{3,1,0,2:T(8,128)S(1)} %bitcast.112), kind=kOutput, calls=%fused_computation.46 | convolution fusion | flops 543162368 | bytes 8404992 | tf_op jit(solution)/shard_map/njhd,njhe->nhde/dot_general | solution.py:100
  56.6 8.1 %while.26 = (s32[]{:T(128)}, f32[2,256,256]{2,1,0:T(8,128)S(1)}, f32[4,2,256,256]{3,2,1,0:T(8,128)}, f32[4,2]{1,0:T(4,128)S(1)}, f32[4,2,256,256]{3,2,1,0:T(8,128)}, /*index=5*/s32[]{:T(128)}, s32[]{:T(128)}) while((s32[]{:T(128)}, f32[2,256,256]{2,1,0:T(8,128)S(1)}, f32[4,2,256,256]{3,2,1,0:T(8,128)}, f32[4,2]{1,0:T(4,128)S(1)}, ...), condition=%wide.region_3.4_spmd.clone, body=%wide.region_2.3_spmd.clone.sunk | while | flops 524291 | bytes 2622072 | solution.py:104
  65.9 20.9 %all-gather.1 = bf16[8,1,2]{2,1,0:T(2,128)(2,1)S(1)} all-gather(bf16[1,1,2]{2,1,0:T(2,128)(2,1)S(1)} %bitcast.127), channel_id=1, replica_groups=mesh['ep'=8,'tp'=4] {'ep'}, dimensions={0}, use_global_device_ids=true | all-gather | bytes 36 | tf_op jit(solution)/shard_map/all_gather | solution.py:31
  89.1 2.9 %copy.142 = bf16[2048,512]{0,1:T(8,128)(2,1)S(1)} copy(bf16[2048,512]{1,0:T(8,128)(2,1)} %param.21) | data formatting | bytes 4194304 | tf_op args[3]
  92.1 7.5 %fusion.14 = f32[4,2,512,256]{3,2,1,0:T(8,128)} fusion(f32[4,2,512]{2,1,0:T(2,128)S(1)} %reshape.302, pred[512,512]{1,0:T(8,128)(4,1)S(1)} %iota_compare_fusion, bf16[4,512,2,256]{3,2,1,0:T(2,128)(2,1)} %reshape.258, f32[4,512,2,128]{3,1,0,2:T(8,128)} %bitcast.114, f32[4,512,2,128]{3,1,0,2:T(8,128)} %bitcast.111, bf16[4,512,2,128]{3,1,0,2:T(8,128)(2,1)} %bitcast.108, ...), kind=kOutput, calls=%fused_computation.26 | convolution fusion | flops 2165309440 | bytes 12861440 | tf_op jit(solution)/shard_map/nhij,njhe->nihe/dot_general | solution.py:93
  99.7 7.8 %fusion.6 = f32[512,1792]{1,0:T(8,128)S(1)} fusion(bf16[512,2048]{1,0:T(8,128)(2,1)} %bitcast.30, bf16[1,2048,1792]{2,1,0:T(8,128)(2,1)} %param.29), kind=kOutput, calls=%fused_computation.16 | convolution fusion | flops 3758096384 | bytes 13107200 | tf_op jit(solution)/shard_map/dot_general | solution.py:157
  107.5 8.1 %multiply_convert_fusion.3 = bf16[512,1792]{1,0:T(8,128)(2,1)S(1)} fusion(f32[512,1792]{1,0:T(8,128)S(1)} %fusion.6, bf16[512,2048]{1,0:T(8,128)(2,1)} %bitcast.30, bf16[1,2048,1792]{2,1,0:T(8,128)(2,1)} %param.30), kind=kOutput, calls=%fused_computation.41 | convolution fusion | flops 3763601408 | bytes 14942208 | tf_op jit(solution)/shard_map/dot_general | solution.py:158
  115.6 4.2 %fusion.31 = bf16[4,8,16,2048]{3,2,0,1:T(8,128)(2,1)S(1)} fusion(bf16[8,4,16,1792]{3,2,1,0:T(8,128)(2,1)S(1)} %bitcast.130, bf16[1,1792,2048]{2,1,0:T(8,128)(2,1)S(1)} %bitcast.129), kind=kOutput, calls=%fused_computation.45 | convolution fusion | flops 3759144960 | bytes 11272192 | tf_op jit(solution)/shard_map/elcf,fd->lecd/dot_general | solution.py:164
  121.7 9.3 %multiply_reduce_fusion = (f32[4,512,2]{1,2,0:T(2,128)S(1)}, f32[4,512,2,256]{3,1,2,0:T(8,128)S(1)}) fusion(f32[4,512,2]{1,2,0:T(2,128)S(1)} %copy.165, f32[4,2,256,256]{3,2,1,0:T(8,128)} %get-tuple-element.74, f32[2,256,256]{2,1,0:T(8,128)S(1)} %get-tuple-element.76, f32[4,2]{1,0:T(4,128)S(1)} %copy.162, f32[4,2,512,256]{3,2,1,0:T(8,128)} %fusion.14, ...), kind=kOutput, calls=%fused_computation.31 | convolution fusion | flops 3231707136 | bytes 13140000 | tf_op jit(solution)/shard_map/nihd,nhde->nihe/dot_general | solution.py:112
  133.2 5.4 %copy.169 = f32[2048,2,256]{0,2,1:T(8,128)} copy(f32[2048,2,256]{2,0,1:T(8,128)} %bitcast.100) | data formatting | bytes 8388608 | tf_op jit(solution)/shard_map/reshape | solution.py:115
  138.7 3.8 %fusion.22 = bf16[2048,2,256]{0,2,1:T(8,128)(2,1)S(1)} fusion(f32[2048,2,256]{0,2,1:T(8,128)} %copy.169, bf16[2048,2,256]{0,2,1:T(8,128)(2,1)S(1)} %bitcast.102, f32[2,256]{1,0:T(2,128)S(1)} %mul.262, f32[2048,2]{0,1:T(2,128)S(1)} %bitcast.122), kind=kLoop, calls=%fused_computation.39 | loop fusion | flops 9437184 | bytes 8407040 | tf_op jit(solution)/shard_map/convert_element_type | solution.py:120
  144.3 3.7 %all-to-all-start = ((bf16[4,512,512]{1,2,0:T(8,128)(2,1)}), bf16[4,512,512]{1,2,0:T(8,128)(2,1)S(1)}, u32[]{:S(2)}, u32[]{:S(2)}) async-start(bf16[4,512,512]{1,2,0:T(8,128)(2,1)} %pad_maximum_fusion.2), calls=%async_computation | async-start | bytes 4194304 | tf_op jit(solution)/shard_map/all_to_all | solution.py:14
  148.1 25.5 %all-to-all-done = bf16[4,512,512]{1,2,0:T(8,128)(2,1)S(1)} async-done(((bf16[4,512,512]{1,2,0:T(8,128)(2,1)}), bf16[4,512,512]{1,2,0:T(8,128)(2,1)S(1)}, u32[]{:S(2)}, u32[]{:S(2)}) %all-to-all-start) | async-done | bytes 2097184 | tf_op jit(solution)/shard_map/all_to_all | solution.py:14
  173.7 10.1 %all-to-all-start.2 = ((bf16[8,16,2048]{2,1,0:T(8,128)(2,1)}), bf16[8,16,2048]{2,1,0:T(8,128)(2,1)S(1)}, u32[]{:S(2)}, u32[]{:S(2)}) async-start(bf16[8,16,2048]{2,1,0:T(8,128)(2,1)} %bitcast.121), calls=%async_computation.3 | async-start | bytes 1048576 | tf_op jit(solution)/shard_map/all_to_all | solution.py:175
  183.8 9.1 %convolution_convert_fusion = bf16[512,2048]{1,0:T(8,128)(2,1)} fusion(bf16[512,2048]{0,1:T(8,128)(2,1)S(1)} %bitcast.115, bf16[2048,2048]{1,0:T(8,128)(2,1)} %param.24), kind=kOutput, calls=%fused_computation.43 | convolution fusion | flops 4296015872 | bytes 12582912 | tf_op jit(solution)/shard_map/dot_general | solution.py:122
  192.9 5.1 %all-to-all-done.2 = bf16[8,16,2048]{2,1,0:T(8,128)(2,1)S(1)} async-done(((bf16[8,16,2048]{2,1,0:T(8,128)(2,1)}), bf16[8,16,2048]{2,1,0:T(8,128)(2,1)S(1)}, u32[]{:S(2)}, u32[]{:S(2)}) %all-to-all-start.2) | async-done | bytes 524320 | tf_op jit(solution)/shard_map/all_to_all | solution.py:175
  (99 shorter events, 33.7 us)
Async XLA Ops:
  15.6 7.5 %copy-start.4 = (f32[2048,2]{0,1:T(2,128)S(1)}, f32[2048,2]{0,1:T(2,128)}, u32[]{:S(2)}) copy-start(f32[2048,2]{0,1:T(2,128)} %param.22) | copy-start | bytes 49156
  15.6 84.1 %all-to-all-start.1 = ((bf16[32,16,2048]{2,1,0:T(8,128)(2,1)}), bf16[32,16,2048]{2,1,0:T(8,128)(2,1)}, u32[]{:S(2)}, u32[]{:S(2)}) async-start(bf16[32,16,2048]{2,1,0:T(8,128)(2,1)} %bitcast.29), calls=%async_computation.1 | async-start | bytes 4194304 | tf_op jit(solution)/shard_map/all_to_all | solution.py:150
  23.0 98.4 %all-gather.4.cloned.1.call-start = ((), (), s32[]{:S(2)}) async-start(), calls=%async_computation.5 | async-start | bytes 2359296 | tf_op jit(solution)/shard_map/all_gather | solution.py:31
  35.2 4.2 %copy-start = (f32[2048,2,256]{0,2,1:T(8,128)S(1)}, f32[2048,2,256]{0,2,1:T(8,128)}, u32[]{:S(2)}) copy-start(f32[2048,2,256]{0,2,1:T(8,128)} %convert.17) | copy-start | bytes 12582916
  47.3 4.2 %copy-start.3 = (f32[2048,2,128]{2,0,1:T(8,128)S(1)}, f32[2048,2,128]{2,0,1:T(8,128)}, u32[]{:S(2)}) copy-start(f32[2048,2,128]{2,0,1:T(8,128)} %copy.149) | copy-start | bytes 6291460
  56.6 30.3 %copy-start.1 = (bf16[2048,2,128]{0,2,1:T(8,128)(2,1)S(1)}, bf16[2048,2,128]{0,2,1:T(8,128)(2,1)}, u32[]{:S(2)}) copy-start(bf16[2048,2,128]{0,2,1:T(8,128)(2,1)} %get-tuple-element.184) | copy-start | bytes 3145732
  65.5 108.2 %reduce-scatter.2.cloned.1.call-start = ((), (), s32[]{:S(2)}) async-start(), calls=%async_computation.4 | async-start | bytes 2621440 | tf_op jit(solution)/shard_map/reduce_scatter | solution.py:167
  87.6 4.6 %copy-start.2 = (bf16[2048,2,128]{2,0,1:T(8,128)(2,1)}, bf16[2048,2,128]{2,0,1:T(8,128)(2,1)S(1)}, u32[]{:S(2)}) copy-start(bf16[2048,2,128]{2,0,1:T(8,128)(2,1)S(1)} %copy.144) | copy-start | bytes 3145732
  89.1 3.0 %copy-start.5 = (f32[512]{0:T(512)S(1)}, f32[512]{0:T(512)}, u32[]{:S(2)}) copy-start(f32[512]{0:T(512)} %param.23) | copy-start | bytes 6148
  99.7 15.9 %slice-start = ((s8[7340032]{0:T(1024)(128)(4,1)}), s8[4194304]{0:T(1024)(128)(4,1)S(1)}, s32[]{:S(2)}) async-start(s8[7340032]{0:T(1024)(128)(4,1)} %bitcast.128), calls=%async_computation.6 | async-start | bytes 8388608
  107.5 8.1 %slice-start.1 = ((s8[7340032]{0:T(1024)(128)(4,1)}), s8[3145728]{0:T(1024)(128)(4,1)S(1)}, s32[]{:S(2)}) async-start(s8[7340032]{0:T(1024)(128)(4,1)} %bitcast.128), calls=%async_computation.7 | async-start | bytes 6291456
  144.3 3.8 %copy-start.6 = (f32[32,2]{0,1:T(2,128)S(1)}, f32[32,2]{0,1:T(2,128)}, u32[]{:S(2)}) copy-start(f32[32,2]{0,1:T(2,128)} %param.27) | copy-start | bytes 772
  144.3 29.4 %all-to-all-start = ((bf16[4,512,512]{1,2,0:T(8,128)(2,1)}), bf16[4,512,512]{1,2,0:T(8,128)(2,1)S(1)}, u32[]{:S(2)}, u32[]{:S(2)}) async-start(bf16[4,512,512]{1,2,0:T(8,128)(2,1)} %pad_maximum_fusion.2), calls=%async_computation | async-start | bytes 4194304 | tf_op jit(solution)/shard_map/all_to_all | solution.py:14
  173.7 24.4 %all-to-all-start.2 = ((bf16[8,16,2048]{2,1,0:T(8,128)(2,1)}), bf16[8,16,2048]{2,1,0:T(8,128)(2,1)S(1)}, u32[]{:S(2)}, u32[]{:S(2)}) async-start(bf16[8,16,2048]{2,1,0:T(8,128)(2,1)} %bitcast.121), calls=%async_computation.3 | async-start | bytes 1048576 | tf_op jit(solution)/shard_map/all_to_all | solution.py:175
Sparse Core Ops, SparseCore 0:
  65.6 50.4 all-gather.3
Sparse Core Ops, SparseCore 1:
  121.5 28.3 reduce-scatter.1
